TPU v7x, 32 devices: a whole 2x2x4 slice. The times are simulated.
32 devices in a mesh: sp: 8 (over z, x), tp: 4 (over y, core).
Axes of the slice: x: 2, y: 2, z: 4, core: 2. Of those that a mesh axis runs over, the one named last changes fastest.
Arguments:
- residual: bfloat16 [2048, 2048], P('sp', 'tp'), may hold values from -48 to 48
- queries: bfloat16 [2048, 1024], P('sp', 'tp'), may hold values from -6 to 6
- key_rows: bfloat16 [2048, 512], P('sp', 'tp'), may hold values from -6 to 6
- value_rows: bfloat16 [2048, 512], P('sp', 'tp'), may hold values from -6 to 6
- break_shift: bfloat16 [4, 2048], P('tp', 'sp'), may hold values from -20 to 0
- head_gain: float32 [1024], P('tp'), may hold values from 0.1 to 1.9
- out_weight: bfloat16 [1024, 2048], P('tp'), may hold values from -0.1875 to 0.1875
- mlp_gain: float32 [2048], replicated, may hold values from 0.1 to 1.9
- up_weight: bfloat16 [2048, 8192], P('sp', 'tp'), may hold values from -0.125 to 0.125
- down_weight: bfloat16 [8192, 2048], P('tp', 'sp'), may hold values from -0.0625 to 0.0625
Outputs:
- layer_out: bfloat16 [2048, 2048], P('sp', 'tp')
All inputs are finite; a program needn't handle non-finite values.
Results may differ from a plain program's by a relative error of at most 0.013.
Values may be sent and summed in bfloat16 or wider, within the bound.
A program may use at most 128 MiB of HBM per device.

v0:
```python
import jax
import jax.numpy as jnp
from jax import lax
from jax.sharding import PartitionSpec as P

HEAD_DIM = 128
eps = 1e-06


def stick_attention(queries, key_all, value_all, shift_all, first_pos, key_block):
    token_count = queries.shape[0]
    kv_local = key_all.shape[1] // HEAD_DIM
    query_local = queries.shape[1] // HEAD_DIM
    group_size = query_local // kv_local
    stacked = queries.reshape(token_count, kv_local, group_size, HEAD_DIM).transpose(1, 2, 0, 3)
    stacked = stacked.reshape(kv_local, group_size * token_count, HEAD_DIM)
    query_pos = first_pos + lax.iota(jnp.int32, group_size * token_count) % token_count
    score_scale = HEAD_DIM ** (-0.5)
    block_count = (first_pos + token_count - 1 + key_block - 1) // key_block

    def one_block(turn_index, state_pair):
        running, broken_after = state_pair
        offset = (block_count - 1 - turn_index) * key_block
        key_block_rows = lax.dynamic_slice_in_dim(key_all, offset, key_block, 0).reshape(
            key_block, kv_local, HEAD_DIM
        )
        value_block_rows = lax.dynamic_slice_in_dim(value_all, offset, key_block, 0).reshape(
            key_block, kv_local, HEAD_DIM
        )
        shift_block = lax.dynamic_slice_in_dim(shift_all, offset, key_block, 1).astype(jnp.float32)
        scores = jnp.einsum(
            "grd,kgd->grk", stacked, key_block_rows, preferred_element_type=jnp.float32
        )
        scores = scores * score_scale + shift_block[:, None, :]
        key_pos = offset + lax.iota(jnp.int32, key_block)
        visible = key_pos[None, None, :] < query_pos[None, :, None]
        broken = jnp.where(visible, jax.nn.log_sigmoid(-scores), 0.0)
        later = lax.cumsum(broken, axis=2, reverse=True) - broken + broken_after[:, :, None]
        weights = jnp.where(visible, jnp.exp(jax.nn.log_sigmoid(scores) + later), 0.0).astype(
            jnp.bfloat16
        )
        running = running + jnp.einsum(
            "grk,kgd->grd", weights, value_block_rows, preferred_element_type=jnp.float32
        )
        return (running, broken_after + jnp.sum(broken, axis=2))

    start_pair = (
        jnp.zeros((kv_local, group_size * token_count, HEAD_DIM), jnp.float32),
        jnp.zeros((kv_local, group_size * token_count), jnp.float32),
    )
    running, broken_after = lax.fori_loop(0, block_count, one_block, start_pair)
    running = running.reshape(kv_local, group_size, token_count, HEAD_DIM).transpose(2, 0, 1, 3)
    return running.reshape(token_count, query_local, HEAD_DIM)


def body(
    residual,
    queries,
    key_rows,
    value_rows,
    break_shift,
    head_gain,
    out_weight,
    mlp_gain,
    up_weight,
    down_weight,
):
    token_count = queries.shape[0]
    first_pos = lax.axis_index("sp") * token_count
    key_all, value_all, shift_all = (
        lax.all_gather(key_rows, "sp", axis=0, tiled=True),
        lax.all_gather(value_rows, "sp", axis=0, tiled=True),
        lax.all_gather(break_shift, "sp", axis=1, tiled=True),
    )
    key_block = min(2048, key_all.shape[0])
    mixed = stick_attention(queries, key_all, value_all, shift_all, first_pos, key_block)
    power = jnp.mean(mixed * mixed, axis=2, keepdims=True)
    attended = (mixed * lax.rsqrt(power + eps) * head_gain.reshape(-1, HEAD_DIM)).astype(
        jnp.bfloat16
    )
    attended = attended.reshape(token_count, -1)
    partial_value = jnp.dot(attended, out_weight, preferred_element_type=jnp.float32)
    column_count = residual.shape[1]
    column_start = lax.axis_index("tp") * column_count
    own_part = lax.dynamic_slice_in_dim(
        partial_value, column_start, column_count, 1
    ) + residual.astype(jnp.float32)
    partial_value = lax.dynamic_update_slice_in_dim(partial_value, own_part, column_start, 1)
    hidden_whole = lax.psum(partial_value, "tp").astype(jnp.bfloat16)
    widened = hidden_whole.astype(jnp.float32)
    inverse = lax.rsqrt(jnp.mean(widened * widened, axis=1, keepdims=True) + eps)
    mlp_in = (widened * inverse * mlp_gain).astype(jnp.bfloat16)
    hidden_state = lax.dynamic_slice_in_dim(hidden_whole, column_start, column_count, 1)
    lifted = jnp.dot(
        mlp_in,
        lax.all_gather(up_weight, "sp", axis=0, tiled=True),
        preferred_element_type=jnp.float32,
    )
    activated = jnp.square(jax.nn.relu(lifted)).astype(jnp.bfloat16)
    expanded = jnp.dot(
        activated,
        lax.all_gather(down_weight, "sp", axis=1, tiled=True),
        preferred_element_type=jnp.float32,
    )
    mlp_total = lax.psum_scatter(
        expanded.astype(jnp.bfloat16), "tp", scatter_dimension=1, tiled=True
    ).astype(jnp.float32)
    return (hidden_state.astype(jnp.float32) + mlp_total).astype(jnp.bfloat16)


def solution(mesh):
    in_specs = (
        P("sp", "tp"),
        P("sp", "tp"),
        P("sp", "tp"),
        P("sp", "tp"),
        P("tp", "sp"),
        P("tp"),
        P("tp", None),
        P(),
        P("sp", "tp"),
        P("tp", "sp"),
    )
    out_specs = P("sp", "tp")
    return jax.shard_map(body, mesh=mesh, in_specs=in_specs, out_specs=out_specs, check_vma=False)
```

profile of v0, /device:TPU:0, one launch (start us, length us, event | category | flops | bytes accessed | tf_op | source)
XLA Modules:
  0.0 312.5 jit_solution(17928566602720874883)
XLA Ops:
  6.5 0.7 all-gather.3.cloned.1.call-update
  7.3 0.0 all-gather.5.cloned.1.call-start
  7.3 0.7 all-gather.5.cloned.1.call-update
  8.0 0.0 reduce-scatter.2.cloned.1.call-start
  8.1 35.3 %all_gather.15 = bf16[2048,128]{1,0:T(8,128)(2,1)S(1)} all-gather(bf16[256,128]{1,0:T(8,128)(2,1)} %param.14), channel_id=1, replica_groups=mesh['sp'=8,'tp'=4] {'sp'}, dimensions={0}, use_global_device_ids=true | all-gather | bytes 589824 | tf_op jit(solution)/shard_map/all_gather | solution.py:71
  43.4 33.5 %all_gather.17 = bf16[2048,128]{1,0:T(8,128)(2,1)S(1)} all-gather(bf16[256,128]{1,0:T(8,128)(2,1)} %param.15), channel_id=1, replica_groups=mesh['sp'=8,'tp'=4] {'sp'}, dimensions={0}, use_global_device_ids=true | all-gather | bytes 589824 | tf_op jit(solution)/shard_map/all_gather | solution.py:72
  76.9 0.9 reshape.144
  77.9 22.0 %all_gather.16 = bf16[1,2048]{1,0:T(2,128)(2,1)S(1)} all-gather(bf16[1,256]{1,0:T(2,128)(2,1)} %param.16), channel_id=1, replica_groups=mesh['sp'=8,'tp'=4] {'sp'}, dimensions={1}, use_global_device_ids=true | all-gather | bytes 4608 | tf_op jit(solution)/shard_map/all_gather | solution.py:73
  99.9 48.2 %while.15 = (s32[]{:T(128)}, f32[1,512,128]{2,1,0:T(8,128)S(1)}, f32[1,512]{1,0:T(1,128)S(1)}, s32[]{:T(128)}, s32[]{:T(128)}, /*index=5*/bf16[1,512,128]{2,1,0:...) while((s32[]{:T(128)}, f32[1,512,128]{2,1,0:T(8,128)S(1)}, ...), condition=%wide.region_4.5_spmd.clone, body=%wide.region_0.4_spmd.clone.sunk | while | flops 709041152 | bytes 81762496 | solution.py:51
  100.0 2.6 fusion.64
  102.6 5.0 %fusion.66 = (f32[512]{0:T(512)S(1)}, f32[64,8,16,128]{3,1,2,0:T(8,128)S(1)}) fusion(f32[2048]{0:T(1024)S(1)} %bitcast.98, f32[512,2048]{1,0:T(8,128)} %fusion.64, s32[512]{0:T(512)S(1)} %fusion.65, s32[2048]{0:T(1024)S(1)} %iota_add_fusion.2), kind=kLoop, calls=%fused_computation.30.clone.1 | loop fusion | flops 12582400 | bytes 8409088 | tf_op jit(solution)/shard_map/while/body/reduce_sum | solution.py:45
  107.7 2.9 copy.47
  110.6 5.6 %copy.48 = f32[1,512,16,128]{1,2,3,0:T(8,128)} copy(f32[1,512,16,128]{3,2,1,0:T(8,128)} %bitcast.92) | data formatting | bytes 8388608 | tf_op jit(solution)/shard_map/reshape.112
  116.2 10.8 %fusion.67 = f32[1,512,16,128]{1,2,3,0:T(8,128)S(1)} fusion(f32[1,512,16,128]{1,2,3,0:T(8,128)} %copy.48), kind=kOutput, calls=%fused_computation.52.clone.1 | output fusion | flops 133169152 | bytes 8388608 | tf_op jit(solution)/shard_map/reduce-window.4
  127.0 1.9 copy-done.1
  128.9 0.1 reduce-window.20
  129.0 0.1 copy.49
  129.2 2.6 broadcast.100
  131.8 5.8 %copy.50 = f32[1,512,16,128]{3,2,1,0:T(8,128)} copy(f32[1,512,16,128]{1,2,3,0:T(8,128)} %copy-done.1) | data formatting | bytes 8388608 | tf_op jit(solution)/shard_map/reduce-window.4
  137.6 10.4 %fusion.68 = f32[1,512,128]{2,1,0:T(8,128)S(1)} fusion(f32[1,512,128]{2,1,0:T(8,128)S(1)} %get-tuple-element.245, bf16[2048,128]{1,0:T(8,128)(2,1)S(1)} %get-tuple-element.265, f32[64,8,16,128]{3,2,1,0:T(8,128)} %bitcast.93, f32[64,8,16,128]{3,2,1,0:T(8,128)} %bitcast.94, f32[512,2048]{1,0:T(8,128)} %fusion.64, f32[512]{0:T(512)S(1)} %bitcast.101, ...), kind=kOutput, calls=%fused_computation.16.clone.1 | convolution fusion | flops 294715392 | bytes 13651968 | tf_op jit(solution)/shard_map/while/body/grk,kgd->grd/dot_general | solution.py:42
  148.2 0.1 copy.23
  148.4 0.1 multiply_reduce_fusion
  148.5 0.1 fusion.38
  148.7 0.5 fusion.41
  149.1 0.0 copy-done.2
  149.2 0.1 add_dynamic-update-slice_fusion
  149.3 40.4 %all-reduce.1 = bf16[256,2048]{1,0:T(8,128)(2,1)} all-reduce(f32[256,2048]{1,0:T(8,128)S(1)} %add_dynamic-update-slice_fusion), channel_id=1, replica_groups=mesh['sp'=8,'tp'=4] {'tp'}, use_global_device_ids=true, to_apply=%region_6.7 | all-reduce | flops 524288 | bytes 3145728 | tf_op jit(solution)/shard_map/psum | solution.py:89
  189.7 1.5 fusion.29
  191.2 78.2 %all-gather.5.cloned.1.call-done = bf16[2048,2048]{1,0:T(8,128)(2,1)} async-done(((bf16[2048,256]{1,0:T(8,128)(2,1)}), bf16[2048,2048]{1,0:T(8,128)(2,1)}) %all-gather.5.cloned.1.call-update) | async-done | bytes 8388624 | tf_op jit(solution)/shard_map/all_gather | solution.py:102
  269.4 11.6 %convolution_convert_fusion = bf16[256,2048]{1,0:T(8,128)(2,1)} fusion(bf16[2048,2048]{1,0:T(8,128)(2,1)} %all-gather.5.cloned.1.call-done, bf16[2048,2048]{1,0:T(8,128)(2,1)} %all-gather.3.cloned.1.call-done, bf16[256,2048]{1,0:T(8,128)(2,1)} %all-reduce.1, f32[2048]{0:T(1024)S(1)} %copy-done.4, f32[256]{0:T(256)S(1)} %add_rsqrt_fusion.1), kind=kOutput, calls=%fused_computation.37 | convolution fusion | flops 4299161600 | bytes 18883584 | tf_op jit(solution)/shard_map/dot_general | solution.py:100
  281.1 23.1 %reduce-scatter.2.cloned.1.call-done = bf16[256,512]{1,0:T(8,128)(2,1)} async-done(((bf16[256,2048]{1,0:T(8,128)(2,1)}), bf16[256,512]{1,0:T(8,128)(2,1)}) %reduce-scatter.2.cloned.1.call-update) | async-done | bytes 262160 | tf_op jit(solution)/shard_map/reduce_scatter | solution.py:105
  304.2 1.8 add_convert_fusion
  (22 shorter events, 0.2 us)
Async XLA Ops:
  6.5 142.1 %copy-start = (bf16[256,2048]{1,0:T(8,128)(2,1)S(1)}, bf16[256,2048]{1,0:T(8,128)(2,1)}, u32[]{:S(2)}) copy-start(bf16[256,2048]{1,0:T(8,128)(2,1)} %param.18) | copy-start | bytes 3145732
  6.5 184.7 %all-gather.3.cloned.1.call-start = ((), (), s32[]{:S(2)}) async-start(), calls=%async_computation.1 | async-start | bytes 9437184 | tf_op jit(solution)/shard_map/all_gather | solution.py:96
  7.3 262.1 %all-gather.5.cloned.1.call-start = ((), (), s32[]{:S(2)}) async-start(), calls=%async_computation.2 | async-start | bytes 9437184 | tf_op jit(solution)/shard_map/all_gather | solution.py:102
  8.0 296.2 %reduce-scatter.2.cloned.1.call-start = ((), (), s32[]{:S(2)}) async-start(), calls=%async_computation.3 | async-start | bytes 1310720 | tf_op jit(solution)/shard_map/reduce_scatter | solution.py:105
  99.9 48.6 %copy-start.3 = (f32[256]{0:T(256)S(1)}, f32[256]{0:T(256)}, u32[]{:S(2)}) copy-start(f32[256]{0:T(256)} %param.17) | copy-start | bytes 3076
  127.0 1.9 copy-start.1
  148.2 1.0 copy-start.2
  148.6 120.8 %copy-start.4 = (f32[2048]{0:T(1024)S(1)}, f32[2048]{0:T(1024)}, u32[]{:S(2)}) copy-start(f32[2048]{0:T(1024)} %param.19) | copy-start | bytes 24580
Sparse Core Ops, SparseCore 0:
  9.5 134.2 all-gather.2
  145.8 123.5 all-gather.4
  281.2 22.9 reduce-scatter.1
where the time goes:
time: 313 us
  blocking collectives  131 us (42%)
  waiting for transfers between devices  103 us (33%)
  matrix products  25.2 us (8%)
  local copies, waits for them, and re-layouts  20.1 us (6%)
  other arithmetic  19.6 us (6%)
  between operations  13.2 us (4%)
    all_gather x1, waiting for transfers between devices, body(): lax.all_gather(down_weight, 'sp', axis=1, tiled=True)  78.2 us
    psum x1, blocking collectives, body(): hidden_whole = lax.psum(partial_value, 'tp').astype(jnp.bfloat16)  40.4 us
    all_gather x1, blocking collectives, body(): lax.all_gather(key_rows, 'sp', axis=0, tiled=True)  35.3 us
    all_gather x1, blocking collectives, body(): lax.all_gather(value_rows, 'sp', axis=0, tiled=True)  33.5 us
    reduce_scatter x1, waiting for transfers between devices, body(): lax.psum_scatter(expanded.astype(jnp.bfloat16), 'tp', scatter_dimension=1...  23.1 us
    all_gather x1, blocking collectives, body(): lax.all_gather(break_shift, 'sp', axis=1, tiled=True)  22 us
    another operation x6, local copies, waits for them, and re-layouts  14.1 us
    dot_general x1, matrix products, body(): jnp.dot(activated, lax.all_gather(down_weight, 'sp', axis=1, tiled=True),...  11.6 us
  transfers between devices with their start and end apart: 3, of which 2 were waited for; matrix products, arithmetic and copies ran while one was open for 16% of the time, Pallas kernels for 0%

commit v1 on v0

--- a/solution.py
+++ b/solution.py
@@ -86,7 +86,7 @@
         partial_value, column_start, column_count, 1
     ) + residual.astype(jnp.float32)
     partial_value = lax.dynamic_update_slice_in_dim(partial_value, own_part, column_start, 1)
-    hidden_whole = lax.psum(partial_value, "tp").astype(jnp.bfloat16)
+    hidden_whole = jnp.sum(lax.all_gather(partial_value, "tp"), axis=0).astype(jnp.bfloat16)
     widened = hidden_whole.astype(jnp.float32)
     inverse = lax.rsqrt(jnp.mean(widened * widened, axis=1, keepdims=True) + eps)
     mlp_in = (widened * inverse * mlp_gain).astype(jnp.bfloat16)

time: 313 us -> 496 us (1.58)
  waiting for transfers between devices: 103 us -> 326 us
  blocking collectives: 131 us -> 85.9 us
    all_gather x1, waiting for transfers between devices: 0.02 us -> 122 us  [body(): lax.all_gather(up_weight, 'sp', axis=0, tiled=True)]
    all_gather x0 -> x1, waiting for transfers between devices: none -> 54.2 us  [body(): lax.all_gather(partial_value, 'tp')]
    all_gather x1, waiting for transfers between devices: 78.2 us -> 125 us  [body(): lax.all_gather(down_weight, 'sp', axis=1, tiled=True)]
    psum x1 -> x0, blocking collectives: 40.4 us -> none  [body(): hidden_whole = lax.psum(partial_value, 'tp').astype(jnp.bfloat16)]
  transfers between devices with their start and end apart: 3 -> 4, of which waited for: 2 -> 4; matrix products, arithmetic and copies ran while one was open for 16% -> 1% of each run, Pallas kernels for 0% -> 0%
where the time goes in v1:
time: 496 us; the launch traced here: 495 us
  waiting for transfers between devices  326 us (66%)
  blocking collectives  85.9 us (17%)
  matrix products  24.8 us (5%)
  other arithmetic  23.6 us (5%)
  local copies, waits for them, and re-layouts  21.5 us (4%)
  between operations  13.2 us (3%)
    all_gather x1, waiting for transfers between devices, body(): lax.all_gather(down_weight, 'sp', axis=1, tiled=True)  125 us
    all_gather x1, waiting for transfers between devices, body(): lax.all_gather(up_weight, 'sp', axis=0, tiled=True)  122 us
    all_gather x1, waiting for transfers between devices, body(): lax.all_gather(partial_value, 'tp')  54.2 us
    all_gather x1, blocking collectives, body(): lax.all_gather(key_rows, 'sp', axis=0, tiled=True)  33.4 us
    all_gather x1, blocking collectives, body(): lax.all_gather(value_rows, 'sp', axis=0, tiled=True)  31.4 us
    reduce_scatter x1, waiting for transfers between devices, body(): lax.psum_scatter(expanded.astype(jnp.bfloat16), 'tp', scatter_dimension=1...  23.1 us
    all_gather x1, blocking collectives, body(): lax.all_gather(break_shift, 'sp', axis=1, tiled=True)  21.1 us
    another operation x6, local copies, waits for them, and re-layouts  14.1 us
  transfers between devices with their start and end apart: 4, of which 4 were waited for; matrix products, arithmetic and copies ran while one was open for 1% of the time, Pallas kernels for 0%

profile of v1, /device:TPU:0, one launch (start us, length us, event | category | flops | bytes accessed | tf_op | source)
XLA Modules:
  0.0 495.2 jit_solution(9299757350554008745)
XLA Ops:
  6.5 33.4 %all_gather.23 = bf16[2048,128]{1,0:T(8,128)(2,1)S(1)} all-gather(bf16[256,128]{1,0:T(8,128)(2,1)} %param.14), channel_id=1, replica_groups=mesh['sp'=8,'tp'=4] {'sp'}, dimensions={0}, use_global_device_ids=true | all-gather | bytes 589824 | tf_op jit(solution)/shard_map/all_gather | solution.py:71
  39.9 31.4 %all_gather.25 = bf16[2048,128]{1,0:T(8,128)(2,1)S(1)} all-gather(bf16[256,128]{1,0:T(8,128)(2,1)} %param.15), channel_id=1, replica_groups=mesh['sp'=8,'tp'=4] {'sp'}, dimensions={0}, use_global_device_ids=true | all-gather | bytes 589824 | tf_op jit(solution)/shard_map/all_gather | solution.py:72
  71.3 0.9 reshape.146
  72.3 21.1 %all_gather.24 = bf16[1,2048]{1,0:T(2,128)(2,1)S(1)} all-gather(bf16[1,256]{1,0:T(2,128)(2,1)} %param.16), channel_id=1, replica_groups=mesh['sp'=8,'tp'=4] {'sp'}, dimensions={1}, use_global_device_ids=true | all-gather | bytes 4608 | tf_op jit(solution)/shard_map/all_gather | solution.py:73
  93.5 48.3 %while.15 = (s32[]{:T(128)}, f32[1,512,128]{2,1,0:T(8,128)S(1)}, f32[1,512]{1,0:T(1,128)S(1)}, s32[]{:T(128)}, s32[]{:T(128)}, /*index=5*/bf16[1,512,128]{2,1,0:...) while((s32[]{:T(128)}, f32[1,512,128]{2,1,0:T(8,128)S(1)}, ...), condition=%wide.region_4.5_spmd.clone, body=%wide.region_0.4_spmd.clone.sunk | while | flops 709041152 | bytes 81762496 | solution.py:51
  93.5 2.6 fusion.64
  96.2 5.0 %fusion.66 = (f32[512]{0:T(512)S(1)}, f32[64,8,16,128]{3,1,2,0:T(8,128)S(1)}) fusion(f32[2048]{0:T(1024)S(1)} %bitcast.102, f32[512,2048]{1,0:T(8,128)} %fusion.64, s32[512]{0:T(512)S(1)} %fusion.65, s32[2048]{0:T(1024)S(1)} %iota_add_fusion.2), kind=kLoop, calls=%fused_computation.30.clone.1 | loop fusion | flops 12582400 | bytes 8409088 | tf_op jit(solution)/shard_map/while/body/reduce_sum | solution.py:45
  101.2 2.9 copy.52
  104.1 5.6 %copy.53 = f32[1,512,16,128]{1,2,3,0:T(8,128)} copy(f32[1,512,16,128]{3,2,1,0:T(8,128)} %bitcast.95) | data formatting | bytes 8388608 | tf_op jit(solution)/shard_map/reshape.114
  109.7 10.8 %fusion.67 = f32[1,512,16,128]{1,2,3,0:T(8,128)S(1)} fusion(f32[1,512,16,128]{1,2,3,0:T(8,128)} %copy.53), kind=kOutput, calls=%fused_computation.52.clone.1 | output fusion | flops 133169152 | bytes 8388608 | tf_op jit(solution)/shard_map/reduce-window.4
  120.5 1.9 copy-done.1
  122.5 0.1 reduce-window.20
  122.6 0.1 copy.54
  122.7 2.6 broadcast.100
  125.3 5.8 %copy.55 = f32[1,512,16,128]{3,2,1,0:T(8,128)} copy(f32[1,512,16,128]{1,2,3,0:T(8,128)} %copy-done.1) | data formatting | bytes 8388608 | tf_op jit(solution)/shard_map/reduce-window.4
  131.1 10.4 %fusion.68 = f32[1,512,128]{2,1,0:T(8,128)S(1)} fusion(f32[1,512,128]{2,1,0:T(8,128)S(1)} %get-tuple-element.245, bf16[2048,128]{1,0:T(8,128)(2,1)S(1)} %get-tuple-element.265, f32[64,8,16,128]{3,2,1,0:T(8,128)} %bitcast.96, f32[64,8,16,128]{3,2,1,0:T(8,128)} %bitcast.97, f32[512,2048]{1,0:T(8,128)} %fusion.64, f32[512]{0:T(512)S(1)} %bitcast.105, ...), kind=kOutput, calls=%fused_computation.16.clone.1 | convolution fusion | flops 294715392 | bytes 13651968 | tf_op jit(solution)/shard_map/while/body/grk,kgd->grd/dot_general | solution.py:42
  141.7 0.1 copy.28
  141.9 0.1 multiply_reduce_fusion
  142.1 0.1 fusion.38
  142.2 0.5 fusion.41
  142.6 1.4 copy.65
  144.0 0.9 bitcast_dynamic-update-slice_fusion
  145.0 0.7 all-gather.6.cloned.1.call-update
  145.8 0.7 all-gather.8.cloned.1.call-update
  146.5 54.2 %all-gather.4.cloned.1.call-done = f32[4,256,2048]{2,1,0:T(8,128)} async-done(((f32[1,256,2048]{2,1,0:T(8,128)}), f32[4,256,2048]{2,1,0:T(8,128)}) %all-gather.4.cloned.1.call-update) | async-done | bytes 8388624 | tf_op jit(solution)/shard_map/all_gather | solution.py:89
  200.7 4.4 reduce_sum.39
  205.1 0.3 fusion.29
  205.4 121.9 %all-gather.6.cloned.1.call-done = bf16[2048,2048]{1,0:T(8,128)(2,1)} async-done(((bf16[256,2048]{1,0:T(8,128)(2,1)}), bf16[2048,2048]{1,0:T(8,128)(2,1)}) %all-gather.6.cloned.1.call-update) | async-done | bytes 8388624 | tf_op jit(solution)/shard_map/all_gather | solution.py:96
  327.3 125.2 %all-gather.8.cloned.1.call-done = bf16[2048,2048]{1,0:T(8,128)(2,1)} async-done(((bf16[2048,256]{1,0:T(8,128)(2,1)}), bf16[2048,2048]{1,0:T(8,128)(2,1)}) %all-gather.8.cloned.1.call-update) | async-done | bytes 8388624 | tf_op jit(solution)/shard_map/all_gather | solution.py:102
  452.5 11.3 %convolution_convert_fusion = bf16[256,2048]{1,0:T(8,128)(2,1)} fusion(bf16[2048,2048]{1,0:T(8,128)(2,1)} %all-gather.8.cloned.1.call-done, bf16[2048,2048]{1,0:T(8,128)(2,1)} %all-gather.6.cloned.1.call-done, bf16[256,2048]{1,0:T(8,128)(2,1)S(1)} %reduce_sum.39, f32[2048]{0:T(1024)S(1)} %copy-done.4, f32[256]{0:T(256)S(1)} %add_rsqrt_fusion.1), kind=kOutput, calls=%fused_computation.37 | convolution fusion | flops 4299161600 | bytes 18883584 | tf_op jit(solution)/shard_map/dot_general | solution.py:100
  463.8 23.1 %reduce-scatter.2.cloned.1.call-done = bf16[256,512]{1,0:T(8,128)(2,1)} async-done(((bf16[256,2048]{1,0:T(8,128)(2,1)}), bf16[256,512]{1,0:T(8,128)(2,1)}) %reduce-scatter.2.cloned.1.call-update) | async-done | bytes 262160 | tf_op jit(solution)/shard_map/reduce_scatter | solution.py:105
  487.0 1.7 add_convert_fusion
  (26 shorter events, 0.3 us)
Async XLA Ops:
  6.5 135.6 %copy-start = (bf16[256,2048]{1,0:T(8,128)(2,1)S(1)}, bf16[256,2048]{1,0:T(8,128)(2,1)}, u32[]{:S(2)}) copy-start(bf16[256,2048]{1,0:T(8,128)(2,1)} %param.18) | copy-start | bytes 3145732
  6.5 194.1 %all-gather.4.cloned.1.call-start = ((), (), s32[]{:S(2)}) async-start(), calls=%async_computation.1 | async-start | bytes 10485760 | tf_op jit(solution)/shard_map/all_gather | solution.py:89
  93.5 48.6 %copy-start.3 = (f32[256]{0:T(256)S(1)}, f32[256]{0:T(256)}, u32[]{:S(2)}) copy-start(f32[256]{0:T(256)} %param.17) | copy-start | bytes 3076
  120.5 2.0 copy-start.1
  141.9 2.2 copy-start.2
  145.0 182.3 %all-gather.6.cloned.1.call-start = ((), (), s32[]{:S(2)}) async-start(), calls=%async_computation.2 | async-start | bytes 9437184 | tf_op jit(solution)/shard_map/all_gather | solution.py:96
  145.7 306.8 %all-gather.8.cloned.1.call-start = ((), (), s32[]{:S(2)}) async-start(), calls=%async_computation.3 | async-start | bytes 9437184 | tf_op jit(solution)/shard_map/all_gather | solution.py:102
  146.5 306.1 %copy-start.4 = (f32[2048]{0:T(1024)S(1)}, f32[2048]{0:T(1024)}, u32[]{:S(2)}) copy-start(f32[2048]{0:T(1024)} %param.19) | copy-start | bytes 24580
  146.5 340.5 %reduce-scatter.2.cloned.1.call-start = ((), (), s32[]{:S(2)}) async-start(), calls=%async_computation.4 | async-start | bytes 1310720 | tf_op jit(solution)/shard_map/reduce_scatter | solution.py:105
Sparse Core Ops, SparseCore 0:
  145.1 55.5 all-gather.3
  202.8 124.4 all-gather.5
  329.4 123.1 all-gather.7
  464.0 22.9 reduce-scatter.1
